TPU v7x, 128 devices: a whole 4x4x4 slice. The times are simulated.
128 devices in a mesh: sp: 64 (over z, y, x), tp: 2 (over core).
Axes of the slice: x: 4, y: 4, z: 4, core: 2. Of those that a mesh axis runs over, the one named last changes fastest.
Arguments:
- wide_inputs: bfloat16 [8192, 512], P('sp', 'tp'), may hold values from -6 to 6
- narrow_inputs: bfloat16 [8192, 512], P('sp', 'tp'), may hold values from -6 to 6
- wide_poles: float32 [2, 2, 32, 64], P(None, None, 'tp'), may hold values from -3.1416 to 3.1416, as said below
- narrow_poles: float32 [2, 2, 32, 32], P(None, None, 'tp'), may hold values from -3.1416 to 3.1416, as said below
- step_sizes: float32 [2, 2, 32], P(None, None, 'tp'), may hold values from 0 to 1, as said below
- forget: float32 [2, 2, 32, 8192], P(None, None, 'tp', 'sp'), may hold values from 0 to 2.2
- wide_in_map: float32 [2, 2, 32, 16, 64], P(None, None, 'tp'), may hold values from -2.5 to 2.5
- narrow_in_map: float32 [2, 2, 32, 16, 32], P(None, None, 'tp'), may hold values from -2.5 to 2.5
- wide_out_map: float32 [2, 2, 32, 16, 64], P(None, None, 'tp'), may hold values from -1.25 to 1.25
- narrow_out_map: float32 [2, 2, 32, 16, 32], P(None, None, 'tp'), may hold values from -2 to 2
- skip_weight: bfloat16 [2, 512], P(None, 'tp'), may hold values from -6 to 6
- gate_mix: bfloat16 [2, 32, 16, 16], P(None, 'tp'), may hold values from -1.5 to 1.5
- residual: bfloat16 [8192, 2048], P(('sp', 'tp')), may hold values from -6 to 6
- mixer_gain: float32 [1024], replicated, may hold values from 0.1 to 1.9
- out_proj: bfloat16 [1024, 2048], replicated, may hold values from -0.1875 to 0.1875
- ffn_gain: float32 [2048], replicated, may hold values from 0.1 to 1.9
- routes: int32 [8192, 2], P(('sp', 'tp')), may hold values from 0 to 127, all different within a row; in each aligned block of 64 rows (0 to 63, 64 to 127, ...) at most 2 rows name the same one
- route_weights: float32 [8192, 2], P(('sp', 'tp')), may hold values from 0.1 to 1
- gate_proj: bfloat16 [128, 2048, 1408], P(('sp', 'tp')), may hold values from -0.125 to 0.125
- up_proj: bfloat16 [128, 2048, 1408], P(('sp', 'tp')), may hold values from -0.125 to 0.125
- down_proj: bfloat16 [128, 1408, 2048], P(('sp', 'tp')), may hold values from -0.15625 to 0.15625
Outputs:
- layer_out: bfloat16 [8192, 2048], P(('sp', 'tp'))
Inputs may be any that keep to these rules, and one draw needn't show every extreme that they name: `routes`: in each aligned block of 64 rows (the rows of one device), no expert is named by more than 2 entries, and the 2 experts of a row differ. `wide_poles`: along dimension 1, entry 0 (the real part) is negative and entry 1 (the imaginary part) is at least 0.1 in magnitude. `narrow_poles`: along dimension 1, entry 0 (the real part) is negative and entry 1 (the imaginary part) is at least 0.1 in magnitude. `step_sizes`: Positive.
All inputs are finite; a program needn't handle non-finite values.
Results may differ from a plain program's by a relative error of at most 0.014.
Values may be sent and summed in bfloat16 or wider, within the bound.
A program may use at most 192 MiB of HBM per device.

v0:
```python
import functools

import jax
import jax.numpy as jnp
from jax import lax
from jax.experimental import pallas as pl
from jax.experimental.pallas import tpu as pltpu
from jax.sharding import PartitionSpec as P

epsilon = 1e-06
SUBLANES = 8
LANES = 128


def complex_power(re, im, exponent):
    out_re, out_im = None, None
    while exponent:
        if exponent & 1:
            if out_re is None:
                out_re, out_im = re, im
            else:
                out_re, out_im = out_re * re - out_im * im, out_re * im + out_im * re
        re, im = re * re - im * im, 2.0 * re * im
        exponent >>= 1
    return out_re, out_im


def packs_of(channels, groups, wide_state, narrow_state):
    per = LANES // channels
    packs, column = [], 0
    for which, states in enumerate((wide_state, narrow_state)):
        for pack in range(groups // per):
            group = which * groups + pack * per
            packs.append((group * channels, column, group, per * states, states))
            column += per * states
    return packs


def spread(rows, channels, states):
    tiled = jnp.concatenate([rows] * (LANES // channels), axis=0)
    row = lax.broadcasted_iota(jnp.int32, tiled.shape, 0) // channels
    column = lax.broadcasted_iota(jnp.int32, tiled.shape, 1) // states
    return jnp.where(row == column, tiled, 0.0).astype(jnp.bfloat16)


def fill_pack(pack, direction, channels, u_ref, in_ref, keep_ref, push_re, push_im, keep):
    channel, column, group, width, states = pack
    signal = u_ref[:, channel : channel + LANES]
    for part, target in enumerate((push_re, push_im)):
        rows = in_ref[direction, part, :, column : column + width]
        target[:, :width] = jnp.dot(
            signal, spread(rows, channels, states), preferred_element_type=jnp.float32
        )
    groups = keep_ref.shape[2]
    row = lax.broadcasted_iota(jnp.int32, (groups, width), 0)
    owner = group + lax.broadcasted_iota(jnp.int32, (groups, width), 1) // states
    keep[:, :width] = jnp.dot(
        keep_ref[direction],
        jnp.where(row == owner, 1.0, 0.0),
        precision=lax.Precision.HIGHEST,
        preferred_element_type=jnp.float32,
    )


def order(count, direction):
    return range(count) if direction == 0 else range(count - 1, -1, -1)


def ends_kernel(packs, channels, u_ref, in_ref, rate_ref, keep_ref, ends_ref, sub_ref, push_re, push_im, keep):
    steps = u_ref.shape[0] // SUBLANES
    for pack in packs:
        _, column, _, width, _ = pack
        cols = slice(column, column + width)
        for direction in range(2):
            fill_pack(pack, direction, channels, u_ref, in_ref, keep_ref, push_re, push_im, keep)
            rate_re = rate_ref[2 * direction : 2 * direction + 1, cols]
            rate_im = rate_ref[2 * direction + 1 : 2 * direction + 2, cols]
            h_re = jnp.zeros((SUBLANES, width), jnp.float32)
            h_im = jnp.zeros((SUBLANES, width), jnp.float32)
            kept = jnp.ones((SUBLANES, width), jnp.float32)
            for step in order(steps, direction):
                rows = slice(step * SUBLANES, (step + 1) * SUBLANES)
                hold = keep[rows, :width]
                new_re = hold * (rate_re * h_re - rate_im * h_im) + push_re[rows, :width]
                h_im = hold * (rate_re * h_im + rate_im * h_re) + push_im[rows, :width]
                h_re = new_re
                kept = kept * hold
            power_re, power_im = complex_power(rate_re, rate_im, steps)
            sub_ref[direction, 0, :, cols] = h_re
            sub_ref[direction, 1, :, cols] = h_im
            sub_ref[direction, 2, :, cols] = kept * power_re
            sub_ref[direction, 3, :, cols] = kept * power_im
            decay_re = kept * power_re
            decay_im = kept * power_im
            e_re = jnp.zeros((1, width), jnp.float32)
            e_im = jnp.zeros((1, width), jnp.float32)
            t_re = jnp.ones((1, width), jnp.float32)
            t_im = jnp.zeros((1, width), jnp.float32)
            for j in order(SUBLANES, direction):
                d_re, d_im = decay_re[j : j + 1], decay_im[j : j + 1]
                e_re, e_im = (
                    d_re * e_re - d_im * e_im + h_re[j : j + 1],
                    d_re * e_im + d_im * e_re + h_im[j : j + 1],
                )
                t_re, t_im = d_re * t_re - d_im * t_im, d_re * t_im + d_im * t_re
            for part, value in enumerate((e_re, e_im, t_re, t_im)):
                row = 4 * direction + part
                ends_ref[row : row + 1, cols] = value


def mix_kernel(
    packs, channels, u_ref, in_ref, rate_ref, keep_ref, sub_ref, all_ref, out_map_ref, skip_ref,
    gate_ref, out_ref, push_re, push_im, keep, carry,
):
    tokens = u_ref.shape[0]
    steps = tokens // SUBLANES
    count = all_ref.shape[0]
    mine = lax.axis_index("sp")
    total_width = all_ref.shape[2]

    def hop(k, state):
        result = []
        for direction in range(2):
            at = k if direction == 0 else count - 1 - k
            use = at < mine if direction == 0 else at > mine
            c_re, c_im = state[2 * direction], state[2 * direction + 1]
            base = 4 * direction
            e_re = all_ref[at, base : base + 1, :]
            e_im = all_ref[at, base + 1 : base + 2, :]
            d_re = all_ref[at, base + 2 : base + 3, :]
            d_im = all_ref[at, base + 3 : base + 4, :]
            result.append(jnp.where(use, d_re * c_re - d_im * c_im + e_re, c_re))
            result.append(jnp.where(use, d_re * c_im + d_im * c_re + e_im, c_im))
        return tuple(result)

    zero = jnp.zeros((1, total_width), jnp.float32)
    entering = lax.fori_loop(0, count, hop, (zero, zero, zero, zero))
    for direction in range(2):
        c_re, c_im = entering[2 * direction], entering[2 * direction + 1]
        for j in order(SUBLANES, direction):
            carry[direction, 0, j : j + 1, :] = c_re
            carry[direction, 1, j : j + 1, :] = c_im
            d_re = sub_ref[direction, 2, j : j + 1, :]
            d_im = sub_ref[direction, 3, j : j + 1, :]
            c_re, c_im = (
                d_re * c_re - d_im * c_im + sub_ref[direction, 0, j : j + 1, :],
                d_re * c_im + d_im * c_re + sub_ref[direction, 1, j : j + 1, :],
            )
    for pack in packs:
        channel, column, _, width, states = pack
        cols = slice(column, column + width)
        lanes = slice(channel, channel + LANES)
        read = None
        for direction in range(2):
            fill_pack(pack, direction, channels, u_ref, in_ref, keep_ref, push_re, push_im, keep)
            rate_re = rate_ref[2 * direction : 2 * direction + 1, cols]
            rate_im = rate_ref[2 * direction + 1 : 2 * direction + 2, cols]
            h_re = carry[direction, 0, :, cols]
            h_im = carry[direction, 1, :, cols]
            for step in order(steps, direction):
                rows = slice(step * SUBLANES, (step + 1) * SUBLANES)
                hold = keep[rows, :width]
                new_re = hold * (rate_re * h_re - rate_im * h_im) + push_re[rows, :width]
                h_im = hold * (rate_re * h_im + rate_im * h_re) + push_im[rows, :width]
                h_re = new_re
                push_re[rows, :width] = h_re
                push_im[rows, :width] = h_im
            for part, source in enumerate((push_re, push_im)):
                rows = out_map_ref[direction, part, :, cols]
                if part:
                    rows = -rows
                term = lax.dot_general(
                    source[:, :width].astype(jnp.bfloat16),
                    spread(rows, channels, states),
                    (((1,), (1,)), ((), ())),
                    preferred_element_type=jnp.float32,
                )
                read = term if read is None else read + term
        shaped = read + skip_ref[:, lanes] * u_ref[:, lanes].astype(jnp.float32)
        active = jax.nn.gelu(shaped, approximate=True)
        gate = spread(gate_ref[:, lanes], channels, channels)
        opened = jax.nn.sigmoid(
            jnp.dot(active.astype(jnp.bfloat16), gate, preferred_element_type=jnp.float32)
        )
        out_ref[:, lanes] = (active * opened).astype(jnp.bfloat16)


def share_kernel(ends_ref, all_ref, send_sem, recv_sem):
    count = lax.axis_size("sp")
    mine = lax.axis_index("sp")
    barrier = pltpu.get_barrier_semaphore()
    for k in range(1, count):
        pl.semaphore_signal(
            barrier,
            inc=1,
            device_id={"sp": lax.rem(mine + k, count)},
            device_id_type=pl.DeviceIdType.MESH,
        )
    pl.semaphore_wait(barrier, count - 1)
    copies = []
    for k in range(1, count):
        copy = pltpu.make_async_remote_copy(
            src_ref=ends_ref,
            dst_ref=all_ref.at[mine],
            send_sem=send_sem.at[k],
            recv_sem=recv_sem.at[k],
            device_id={"sp": lax.rem(mine + k, count)},
            device_id_type=pl.DeviceIdType.MESH,
        )
        copy.start()
        copies.append(copy)
    all_ref[mine] = ends_ref[...]
    for copy in copies:
        copy.wait()


def share_ends(ends):
    count = lax.axis_size("sp")
    vmem = pl.BlockSpec(memory_space=pltpu.VMEM)
    return pl.pallas_call(
        share_kernel,
        out_shape=jax.ShapeDtypeStruct((count,) + ends.shape, ends.dtype),
        in_specs=[vmem],
        out_specs=vmem,
        scratch_shapes=[pltpu.SemaphoreType.DMA((count,)), pltpu.SemaphoreType.DMA((count,))],
        compiler_params=pltpu.CompilerParams(collective_id=0, has_side_effects=True),
        name="share_ends",
    )(ends)


def entering_map(poles, step, in_map):
    re, im = poles[:, 0], poles[:, 1]
    growth = jnp.exp(re)
    rate = jnp.stack([growth * jnp.cos(im), growth * jnp.sin(im)], axis=1)
    numer_re = rate[:, 0] - 1.0
    numer_im = rate[:, 1]
    denom = re * re + im * im
    factor_re = ((numer_re * re + numer_im * im) / denom * step[:, :, None])[:, None]
    factor_im = ((numer_im * re - numer_re * im) / denom * step[:, :, None])[:, None]
    moved = jnp.transpose(in_map, (0, 1, 3, 2, 4))
    enter = jnp.stack(
        [
            factor_re * moved[:, 0] - factor_im * moved[:, 1],
            factor_re * moved[:, 1] + factor_im * moved[:, 0],
        ],
        axis=1,
    )
    return rate.reshape(4, -1), enter.reshape(enter.shape[:3] + (-1,))


def mixer(
    wide_inputs, narrow_inputs, wide_poles, narrow_poles, step_sizes, forget, wide_in_map,
    narrow_in_map, wide_out_map, narrow_out_map, skip_weight, gate_mix,
):
    tokens, width = wide_inputs.shape
    groups, channels, wide_state = wide_in_map.shape[2:]
    narrow_state = narrow_in_map.shape[4]
    packs = packs_of(channels, groups, wide_state, narrow_state)
    steps = tokens // SUBLANES
    total = groups * (wide_state + narrow_state)
    widest = max(pack[3] for pack in packs)

    def weave(rows):
        return jnp.swapaxes(rows.reshape(SUBLANES, steps, -1), 0, 1).reshape(tokens, -1)

    signal = weave(jnp.concatenate([wide_inputs, narrow_inputs], axis=1))
    held = jnp.exp(-forget).reshape(2, 2 * groups, SUBLANES, steps)
    held = jnp.transpose(held, (0, 3, 2, 1)).reshape(2, tokens, 2 * groups)
    wide_rate, wide_enter = entering_map(wide_poles, step_sizes[:, 0], wide_in_map)
    narrow_rate, narrow_enter = entering_map(narrow_poles, step_sizes[:, 1], narrow_in_map)
    rate = jnp.concatenate([wide_rate, narrow_rate], axis=1)
    enter = jnp.concatenate([wide_enter, narrow_enter], axis=3)
    leave = jnp.concatenate(
        [
            jnp.transpose(each, (0, 1, 3, 2, 4)).reshape(2, 2, channels, -1)
            for each in (wide_out_map, narrow_out_map)
        ],
        axis=3,
    )
    skip = skip_weight.astype(jnp.float32).reshape(1, -1)
    gate = jnp.transpose(gate_mix.astype(jnp.float32), (2, 0, 1, 3)).reshape(channels, -1)
    vmem = pl.BlockSpec(memory_space=pltpu.VMEM)
    scratch = [pltpu.VMEM((tokens, widest), jnp.float32) for _ in range(3)]
    ends, sub = pl.pallas_call(
        functools.partial(ends_kernel, packs, channels),
        out_shape=(
            jax.ShapeDtypeStruct((8, total), jnp.float32),
            jax.ShapeDtypeStruct((2, 4, SUBLANES, total), jnp.float32),
        ),
        in_specs=[vmem] * 4,
        out_specs=(vmem, vmem),
        scratch_shapes=scratch,
        name="ends",
    )(signal, enter, rate, held)
    gathered = share_ends(ends)
    mixed = pl.pallas_call(
        functools.partial(mix_kernel, packs, channels),
        out_shape=jax.ShapeDtypeStruct((tokens, 2 * width), jnp.bfloat16),
        in_specs=[vmem] * 9,
        out_specs=vmem,
        scratch_shapes=scratch + [pltpu.VMEM((2, 2, SUBLANES, total), jnp.float32)],
        name="mix",
    )(signal, enter, rate, held, sub, gathered, leave, skip, gate)
    return jnp.swapaxes(mixed.reshape(steps, SUBLANES, -1), 0, 1).reshape(tokens, -1)


def local(
    wide_inputs, narrow_inputs, wide_poles, narrow_poles, step_sizes, forget, wide_in_map,
    narrow_in_map, wide_out_map, narrow_out_map, skip_weight, gate_mix, residual, mixer_gain,
    out_proj, ffn_gain, routes, route_weights, gate_proj, up_proj, down_proj,
):
    n_sp = lax.axis_size("sp")
    n_tp = lax.axis_size("tp")
    tp = lax.axis_index("tp")
    set_out = mixer(
        wide_inputs, narrow_inputs, wide_poles, narrow_poles, step_sizes, forget, wide_in_map,
        narrow_in_map, wide_out_map, narrow_out_map, skip_weight, gate_mix,
    )
    tokens = set_out.shape[0]
    rows = tokens // n_tp
    half = set_out.shape[1] // 2
    swapped = lax.all_to_all(
        set_out.reshape(n_tp, rows, -1), "tp", split_axis=0, concat_axis=0, tiled=True
    )
    joined = jnp.concatenate(
        [swapped[k, :, :half] for k in range(n_tp)] + [swapped[k, :, half:] for k in range(n_tp)],
        axis=1,
    ).astype(jnp.float32)
    scale = lax.rsqrt(jnp.mean(joined * joined, axis=1, keepdims=True) + epsilon)
    mixed = (joined * scale * mixer_gain).astype(jnp.bfloat16)
    projected = jnp.dot(mixed, out_proj, preferred_element_type=jnp.float32)
    hidden1 = (residual.astype(jnp.float32) + projected).astype(jnp.bfloat16)
    hidden_wide = hidden1.astype(jnp.float32)
    normed = (
        hidden_wide
        * lax.rsqrt(jnp.mean(hidden_wide * hidden_wide, axis=1, keepdims=True) + epsilon)
        * ffn_gain
    ).astype(jnp.bfloat16)

    experts = n_sp * n_tp
    capacity = 4 * tokens // (n_tp * experts)
    top_count = routes.shape[1]
    width = normed.shape[1]
    slots = experts * capacity
    picks = routes.reshape(-1)
    entries = picks.shape[0]
    onehot = (picks[:, None] == jnp.arange(experts, dtype=jnp.int32)[None, :]).astype(jnp.bfloat16)
    earlier = (
        jnp.arange(entries)[None, :] < jnp.arange(entries)[:, None]
    ).astype(jnp.bfloat16)
    before = jnp.dot(earlier, onehot, preferred_element_type=jnp.float32)
    rank = jnp.sum(before * onehot.astype(jnp.float32), axis=1).astype(jnp.int32)
    place = (picks * capacity + rank).reshape(-1, top_count)
    hit = place[:, :, None] == jnp.arange(slots, dtype=jnp.int32)[None, None, :]
    share = route_weights / jnp.sum(route_weights, axis=1, keepdims=True)
    spot = jnp.any(hit, axis=1).astype(jnp.bfloat16)
    weight = jnp.sum(jnp.where(hit, share[:, :, None], 0.0), axis=1)
    high = lax.reduce_precision(weight, 8, 7)
    weights = jnp.concatenate([high, weight - high], axis=0).astype(jnp.bfloat16)

    sectioning = lax.dot_general(
        spot, normed, (((0,), (0,)), ((), ())), preferred_element_type=jnp.float32
    ).astype(jnp.bfloat16)
    received = lax.all_to_all(
        sectioning.reshape(experts, capacity, width),
        ("sp", "tp"),
        split_axis=0,
        concat_axis=0,
        tiled=True,
    )
    flat_rows = received.reshape(-1, width)
    gate_val = jnp.dot(flat_rows, gate_proj[0], preferred_element_type=jnp.float32)
    up_val = jnp.dot(flat_rows, up_proj[0], preferred_element_type=jnp.float32)
    expert_hidden = (jax.nn.silu(gate_val) * up_val).astype(jnp.bfloat16)
    done = jnp.dot(expert_hidden, down_proj[0], preferred_element_type=jnp.float32).astype(
        jnp.bfloat16
    )
    returned = lax.all_to_all(
        done.reshape(received.shape), ("sp", "tp"), split_axis=0, concat_axis=0, tiled=True
    )
    summed = jnp.dot(weights, returned.reshape(-1, width), preferred_element_type=jnp.float32)
    own = residual.shape[0]
    return (hidden_wide + (summed[:own] + summed[own:])).astype(jnp.bfloat16)


def solution(mesh):
    return jax.shard_map(
        local,
        mesh=mesh,
        in_specs=(
            P("sp", "tp"),
            P("sp", "tp"),
            P(None, None, "tp", None),
            P(None, None, "tp", None),
            P(None, None, "tp"),
            P(None, None, "tp", "sp"),
            P(None, None, "tp", None, None),
            P(None, None, "tp", None, None),
            P(None, None, "tp", None, None),
            P(None, None, "tp", None, None),
            P(None, "tp"),
            P(None, "tp", None, None),
            P(("sp", "tp"), None),
            P(),
            P(),
            P(),
            P(("sp", "tp"), None),
            P(("sp", "tp"), None),
            P(("sp", "tp"), None, None),
            P(("sp", "tp"), None, None),
            P(("sp", "tp"), None, None),
        ),
        out_specs=P(("sp", "tp"), None),
        check_vma=False,
    )
```

profile of v0, /device:TPU:1, one launch (start us, length us, event | category | flops | bytes accessed | tf_op | source)
XLA Modules:
  0.0 165.7 jit_solution(3413760832016247885)
XLA Ops:
  0.0 0.8 fusion.42
  0.8 0.8 multiply_bitcast_fusion.1
  1.6 0.8 multiply_bitcast_fusion
  2.4 0.8 multiply_bitcast_fusion.3
  3.2 0.8 multiply_bitcast_fusion.2
  4.1 0.7 convert_bitcast_fusion.1
  4.8 0.6 copy.75
  5.4 0.8 negate_exponential_fusion
  6.3 0.9 pad_maximum_fusion.1
  7.2 0.7 copy.77
  8.1 0.8 copy.68
  8.9 0.9 convert_bitcast_fusion
  9.9 0.8 reshape.107.gate_ref
  10.7 1.1 multiply_subtract_fusion.1
  13.5 0.9 maximum_maximum_fusion
  14.4 4.0 %ends.1 = (f32[8,1536]{1,0:T(8,128)}, f32[2,4,8,1536]{3,2,1,0:T(8,128)}) custom-call(bf16[128,512]{1,0:T(8,128)(2,1)} %bitcast.92, f32[2,2,16,1536]{3,2,1,0:T(8,128)} %get-tuple-element.29.in_ref, f32[4,1536]{1,0:T(4,128)} %copy-done.4, f32[2,128,32]{2,1,0:T(8,128)} %bitcast.90), custom_call_target="tpu_custom_call" | custom-call | tf_op jit(solution)/shard_map/ends/pallas_call | solution.py:284
  18.4 59.2 %share_ends.1.all_ref = f32[64,8,1536]{2,1,0:T(8,128)} custom-call(f32[8,1536]{1,0:T(8,128)} %get-tuple-element.8.ends_ref), custom_call_target="tpu_custom_call" | custom-call | tf_op jit(solution)/shard_map/share_ends/pallas_call | solution.py:220
  77.7 8.2 %mix.1 = bf16[128,512]{1,0:T(8,128)(2,1)} custom-call(bf16[128,512]{1,0:T(8,128)(2,1)} %bitcast.93, f32[2,2,16,1536]{3,2,1,0:T(8,128)} %get-tuple-element.29.in_ref, f32[4,1536]{1,0:T(4,128)} %copy-done.4, f32[2,128,32]{2,1,0:T(8,128)} %bitcast.91, f32[2,4,8,1536]{3,2,1,0:T(8,128)} %get-tuple-element.7.sub_ref, f32[64,8,1536]{2,1,0:T(8,128)} %share_ends.1.all_ref, ...), custom_call_target="tpu_custom_call" | custom-call | tf_op jit(solution)/shard_map/mix/pallas_call | solution.py:296
  85.9 1.6 copy.72
  87.5 4.9 %all-to-all-start = ((bf16[2,64,512]{2,1,0:T(8,128)(2,1)}), bf16[2,64,512]{2,1,0:T(8,128)(2,1)S(1)}, u32[]{:S(2)}, u32[]{:S(2)}) async-start(bf16[2,64,512]{2,1,0:T(8,128)(2,1)} %bitcast.19), calls=%async_computation | async-start | bytes 262144 | tf_op jit(solution)/shard_map/all_to_all | solution.py:322
  93.7 3.2 %multiply_reduce_fusion = (f32[64]{0:T(128)S(1)}, f32[64,2048]{1,0:T(8,128)S(1)}) fusion(bf16[1024,2048]{1,0:T(8,128)(2,1)} %param.35, f32[1024]{0:T(1024)S(1)} %copy-done.6, f32[64]{0:T(128)S(1)} %add_rsqrt_fusion.1, bf16[64,256]{1,0:T(8,128)(2,1)S(1)} %get-tuple-element.20, bf16[64,256]{1,0:T(8,128)(2,1)S(1)} %get-tuple-element.21, ...), kind=kOutput, calls=%fused_computation.20 | convolution fusion | flops 269942720 | bytes 5116416 | tf_op jit(solution)/shard_map/dot_general | solution.py:331
  96.9 0.5 convolution_convert_fusion
  97.4 0.7 reshape.100
  98.1 26.6 %all_to_all.15 = bf16[128,2,2048]{2,1,0:T(2,128)(2,1)S(1)} all-to-all(bf16[128,2,2048]{2,1,0:T(2,128)(2,1)S(1)} %reshape.100), channel_id=1, replica_groups=mesh['sp'=64,'tp'=2] {'sp','tp'}, dimensions={0} | all-to-all | bytes 2097152 | tf_op jit(solution)/shard_map/all_to_all | solution.py:364
  124.7 0.4 reshape.101
  125.2 5.6 %fusion.4 = f32[256,1408]{1,0:T(8,128)} fusion(bf16[256,2048]{1,0:T(8,128)(2,1)S(1)} %reshape.101, bf16[1,2048,1408]{2,1,0:T(8,128)(2,1)} %param.39), kind=kOutput, calls=%fused_computation.4 | convolution fusion | flops 1476395008 | bytes 8257536 | tf_op jit(solution)/shard_map/dot_general | solution.py:372
  130.7 8.2 %fusion.12 = bf16[256,2048]{1,0:T(8,128)(2,1)S(1)} fusion(bf16[1,1408,2048]{2,1,0:T(8,128)(2,1)} %param.41, bf16[256,2048]{1,0:T(8,128)(2,1)S(1)} %reshape.101, bf16[1,2048,1408]{2,1,0:T(8,128)(2,1)} %param.40, f32[256,1408]{1,0:T(8,128)} %fusion.4), kind=kOutput, calls=%fused_computation.8 | convolution fusion | flops 2955476992 | bytes 15073280 | tf_op jit(solution)/shard_map/dot_general | solution.py:375
  138.9 1.5 reshape.102
  140.4 4.4 %all-to-all-start.2 = ((bf16[128,2,2048]{2,1,0:T(2,128)(2,1)}), bf16[128,2,2048]{2,1,0:T(2,128)(2,1)S(1)}, u32[]{:S(2)}, u32[]{:S(2)}) async-start(bf16[128,2,2048]{2,1,0:T(2,128)(2,1)} %reshape.102), calls=%async_computation.2 | async-start | bytes 2097152 | tf_op jit(solution)/shard_map/all_to_all | solution.py:378
  145.0 19.2 %all-to-all-done.2 = bf16[128,2,2048]{2,1,0:T(2,128)(2,1)S(1)} async-done(((bf16[128,2,2048]{2,1,0:T(2,128)(2,1)}), bf16[128,2,2048]{2,1,0:T(2,128)(2,1)S(1)}, u32[]{:S(2)}, u32[]{:S(2)}) %all-to-all-start.2) | async-done | bytes 1048608 | tf_op jit(solution)/shard_map/all_to_all | solution.py:378
  164.2 0.4 reshape.103
  164.9 0.8 fusion.22
  (57 shorter events, 3.8 us)
Async XLA Ops:
  0.0 12.2 %copy-start = (f32[2,2,16,16,32]{4,3,2,1,0:T(8,128)S(1)}, f32[2,2,16,16,32]{4,3,2,1,0:T(8,128)}, u32[]{:S(2)}) copy-start(f32[2,2,16,16,32]{4,3,2,1,0:T(8,128)} %param.28) | copy-start | bytes 393220
  4.0 8.7 %copy-start.1 = (f32[2,2,16,16,64]{4,3,2,1,0:T(8,128)S(1)}, f32[2,2,16,16,64]{4,3,2,1,0:T(8,128)}, u32[]{:S(2)}) copy-start(f32[2,2,16,16,64]{4,3,2,1,0:T(8,128)} %param.29) | copy-start | bytes 786436
  9.8 3.3 %copy-start.2 = (f32[2,2,16,16,32]{4,3,2,1,0:T(8,128)S(1)}, f32[2,2,16,16,32]{4,3,2,1,0:T(8,128)}, u32[]{:S(2)}) copy-start(f32[2,2,16,16,32]{4,3,2,1,0:T(8,128)} %param.30) | copy-start | bytes 393220
  13.5 0.9 copy-start.4
  18.4 74.0 %copy-start.7 = (s32[64,2]{0,1:T(2,128)S(1)}, s32[64,2]{0,1:T(2,128)}, u32[]{:S(2)}) copy-start(s32[64,2]{0,1:T(2,128)} %param.37) | copy-start | bytes 1540
  18.4 75.2 %copy-start.3 = (bf16[64,2048]{1,0:T(8,128)(2,1)S(1)}, bf16[64,2048]{1,0:T(8,128)(2,1)}, u32[]{:S(2)}) copy-start(bf16[64,2048]{1,0:T(8,128)(2,1)} %param.33) | copy-start | bytes 786436
  18.4 75.2 %copy-start.6 = (f32[1024]{0:T(1024)S(1)}, f32[1024]{0:T(1024)}, u32[]{:S(2)}) copy-start(f32[1024]{0:T(1024)} %param.34) | copy-start | bytes 12292
  85.9 11.0 %copy-start.5 = (f32[2048]{0:T(1024)S(1)}, f32[2048]{0:T(1024)}, u32[]{:S(2)}) copy-start(f32[2048]{0:T(1024)} %param.36) | copy-start | bytes 24580
  87.5 6.0 %all-to-all-start = ((bf16[2,64,512]{2,1,0:T(8,128)(2,1)}), bf16[2,64,512]{2,1,0:T(8,128)(2,1)S(1)}, u32[]{:S(2)}, u32[]{:S(2)}) async-start(bf16[2,64,512]{2,1,0:T(8,128)(2,1)} %bitcast.19), calls=%async_computation | async-start | bytes 262144 | tf_op jit(solution)/shard_map/all_to_all | solution.py:322
  138.9 5.9 %copy-start.8 = (f32[64,2]{0,1:T(2,128)S(1)}, f32[64,2]{0,1:T(2,128)}, u32[]{:S(2)}) copy-start(f32[64,2]{0,1:T(2,128)} %param.38) | copy-start | bytes 1540
  140.4 23.8 %all-to-all-start.2 = ((bf16[128,2,2048]{2,1,0:T(2,128)(2,1)}), bf16[128,2,2048]{2,1,0:T(2,128)(2,1)S(1)}, u32[]{:S(2)}, u32[]{:S(2)}) async-start(bf16[128,2,2048]{2,1,0:T(2,128)(2,1)} %reshape.102), calls=%async_computation.2 | async-start | bytes 2097152 | tf_op jit(solution)/shard_map/all_to_all | solution.py:378
where the time goes:
time: 167 us; the launch traced here: 166 us
  Pallas kernels  71.4 us (43%)
  blocking collectives  26.6 us (16%)
  waiting for transfers between devices  19.5 us (12%)
  matrix products  18 us (11%)
  local copies, waits for them, and re-layouts  10.8 us (6%)
  other arithmetic  9.86 us (6%)
  starting transfers between devices  9.33 us (6%)
    pallas_call x1, Pallas kernels, share_ends(): pl.pallas_call(share_kernel, out_shape=jax.ShapeDtypeStruct((count,) + en...  59.2 us
    all_to_all x1, blocking collectives, local(): lax.all_to_all(sectioning.reshape(experts, capacity, width), ('sp', 'tp')...  26.6 us
    all_to_all x1, waiting for transfers between devices, local(): lax.all_to_all(done.reshape(received.shape), ('sp', 'tp'), split_axis=0,...  19.2 us
    pallas_call x1, Pallas kernels, mixer(): pl.pallas_call(functools.partial(mix_kernel, packs, channels), out_shape=...  8.2 us
    dot_general x1, matrix products, local(): jnp.dot(expert_hidden, down_proj[0], preferred_element_type=jnp.float32)  8.19 us
    dot_general x1, matrix products, local(): jnp.dot(flat_rows, gate_proj[0], preferred_element_type=jnp.float32)  5.55 us
    all_to_all x1, starting transfers between devices, local(): lax.all_to_all(set_out.reshape(n_tp, rows, -1), 'tp', split_axis=0, conca...  4.9 us
    all_to_all x1, starting transfers between devices, local(): lax.all_to_all(done.reshape(received.shape), ('sp', 'tp'), split_axis=0,...  4.43 us
  transfers between devices with their start and end apart: 2, of which 2 were waited for; matrix products, arithmetic and copies ran while one was open for 1% of the time, Pallas kernels for 0%

commit v1 on v0

v1 whole, which is shorter than its diff:
```python
import functools

import jax
import jax.numpy as jnp
from jax import lax
from jax.experimental import pallas as pl
from jax.experimental.pallas import tpu as pltpu
from jax.sharding import PartitionSpec as P

epsilon = 1e-06
SIDE = 4
SUB = 8
LANES = 128
EXACT = lax.Precision.HIGHEST
F32 = jnp.float32
BF16 = jnp.bfloat16
MESH = pl.DeviceIdType.MESH


def iota(shape, dim):
    return lax.broadcasted_iota(jnp.int32, shape, dim)


def ones_where(mask, dtype=F32):
    return jnp.where(mask, 1.0, 0.0).astype(dtype)


def dot(a, b, contract=((1,), (0,)), precision=None):
    return lax.dot_general(a, b, (contract, ((), ())), precision=precision, preferred_element_type=F32)


def sine_cosine(angle):
    y = angle * 0.25
    q = y * y
    s = y * (1.0 + q * (-1 / 6 + q * (1 / 120 + q * (-1 / 5040 + q * (1 / 362880)))))
    c = 1.0 + q * (-0.5 + q * (1 / 24 + q * (-1 / 720 + q * (1 / 40320 + q * (-1 / 3628800)))))
    for _ in range(2):
        s, c = 2.0 * s * c, 1.0 - 2.0 * s * s
    return s, c


def square(re, im):
    return re * re - im * im, 2.0 * re * im


def times(a, b):
    return a[0] * b[0] - a[1] * b[1], a[0] * b[1] + a[1] * b[0]


def plus(a, b):
    return a[0] + b[0], a[1] + b[1]


def spread(rows, mask):
    copies = mask.shape[1] // rows.shape[1]
    tiled = jnp.concatenate([rows] * copies, axis=1)
    return jnp.where(mask, tiled, 0.0).astype(BF16)


def steps_of(count, direction):
    return range(count) if direction == 0 else range(count - 1, -1, -1)


def layer_kernel(
    wide_u, narrow_u, wide_poles, narrow_poles, step_sizes, forget, wide_in, narrow_in, wide_out,
    narrow_out, skip, gate_mix, residual, mixer_gain, ffn_gain, routes, route_weights, out_proj,
    gate_proj, up_proj, down_proj,
    out_ref,
    proj_v, gate_v, up_v, down_v, push, scaled, shrink, plain, leave, gates, ends, before, recv_ends,
    msg, states, woven, halves, pair, sec, arrived, rows_v, hidden_v, served, returned,
    weight_sem, scan_send, scan_recv, pair_sem, send_sem, recv_sem, back_send, back_recv, self_sem,
):
    n_sp = lax.axis_size("sp")
    sp = lax.axis_index("sp")
    tp = lax.axis_index("tp")
    mine = sp * 2 + tp
    n_dev = n_sp * 2

    barrier = pltpu.get_barrier_semaphore()

    def greet(k, _):
        other = lax.rem(mine + k, n_dev)
        pl.semaphore_signal(
            barrier, inc=1, device_id={"sp": other // 2, "tp": lax.rem(other, 2)}, device_id_type=MESH
        )
        return 0

    lax.fori_loop(1, n_dev, greet, 0)
    fetches = [
        pltpu.make_async_copy(source, target, weight_sem.at[i])
        for i, (source, target) in enumerate(
            ((out_proj, proj_v), (gate_proj.at[0], gate_v), (up_proj.at[0], up_v), (down_proj.at[0], down_v))
        )
    ]
    for fetch in fetches:
        fetch.start()

    tokens = wide_u.shape[0]
    steps = tokens // SUB
    sets = (
        (wide_u, wide_poles, wide_in, wide_out),
        (narrow_u, narrow_poles, narrow_in, narrow_out),
    )
    groups, channels = wide_in.shape[2], wide_in.shape[3]
    width = groups * channels
    per = LANES // channels
    states_of = [each[2].shape[4] for each in sets]
    bases = [0, groups * states_of[0]]
    total = groups * sum(states_of)
    packs = []
    for s in range(2):
        for q in range(groups // per):
            packs.append((s, q, s * width + q * LANES, bases[s] + q * per * states_of[s], per * states_of[s]))

    row = iota((tokens, tokens), 0)
    col = iota((tokens, tokens), 1)
    weave = ones_where(col == lax.rem(row, SUB) * steps + row // SUB, BF16)
    unweave = ones_where(col == lax.rem(row, steps) * SUB + row // steps, BF16)
    same = (col // steps) == lax.rem(row, SUB)
    reach = (
        ones_where(same & (lax.rem(col, steps) <= row // SUB)),
        ones_where(same & (lax.rem(col, steps) >= row // SUB)),
    )
    for s in range(2):
        plain[:, s * width : (s + 1) * width] = dot(weave, sets[s][0][...])
    to_channel = ones_where(iota((2 * groups, 2 * width), 0) == iota((2 * groups, 2 * width), 1) // channels)
    lane = iota((2 * groups, total), 1)
    owner = jnp.where(
        lane < bases[1], lane // states_of[0], groups + (lane - bases[1]) // states_of[1]
    )
    to_lane = ones_where(iota((2 * groups, total), 0) == owner)
    kept = []
    for d in range(2):
        flat = forget[d].reshape(2 * groups, tokens)
        lost = dot(reach[d], flat, ((1,), (1,)), EXACT)
        wide = dot(lost, to_channel, precision=EXACT)
        shrink[d] = jnp.exp(-wide)
        scaled[d] = (plain[...] * jnp.exp(wide)).astype(BF16)
        last = lost[tokens - SUB :] if d == 0 else lost[:SUB]
        kept.append(jnp.exp(-dot(last, to_lane, precision=EXACT)))

    masks = [
        (iota((LANES, per * st), 0) // channels) == (iota((LANES, per * st), 1) // st) for st in states_of
    ]
    eye = iota((groups, groups), 0) == iota((groups, groups), 1)
    rates = [[], []]
    for s in range(2):
        _, poles, in_map, out_map = sets[s]
        st = states_of[s]
        for d in range(2):
            re, im = poles[d, 0], poles[d, 1]
            growth = jnp.exp(re)
            sine, cosine = sine_cosine(im)
            rate = (growth * cosine, growth * sine)
            numer_re, numer_im = rate[0] - 1.0, rate[1]
            step = jnp.sum(jnp.where(eye, step_sizes[d, s : s + 1, :], 0.0), axis=1, keepdims=True)
            over = step / (re * re + im * im)
            factor_re = (numer_re * re + numer_im * im) * over
            factor_im = (numer_im * re - numer_re * im) * over
            flat_mask = iota((groups, groups * st), 0) == iota((groups, groups * st), 1) // st
            rates[d].append(
                [
                    jnp.sum(
                        jnp.where(flat_mask, jnp.concatenate([part] * groups, axis=1), 0.0),
                        axis=0,
                        keepdims=True,
                    )
                    for part in rate
                ]
            )
            m_re, m_im = in_map[d, 0], in_map[d, 1]
            f_re, f_im = factor_re[:, None, :], factor_im[:, None, :]
            enter = (
                (f_re * m_re - f_im * m_im).reshape(width, st),
                (f_re * m_im + f_im * m_re).reshape(width, st),
            )
            for which, q, chan, column, lanes in packs:
                if which != s:
                    continue
                for part in range(2):
                    push[d, part, :, column : column + lanes] = dot(
                        scaled[d, :, chan : chan + LANES],
                        spread(enter[part][q * LANES : (q + 1) * LANES], masks[s]),
                    )
    rate_all = [
        [jnp.concatenate([rates[d][0][part], rates[d][1][part]], axis=1) for part in range(2)]
        for d in range(2)
    ]

    for _, _, _, column, lanes in packs:
        cols = slice(column, column + lanes)
        for d in range(2):
            r_re, r_im = rate_all[d][0][:, cols], rate_all[d][1][:, cols]
            h_re = h_im = None
            for step in steps_of(steps, d):
                at = slice(step * SUB, (step + 1) * SUB)
                p_re, p_im = push[d, 0, at, cols], push[d, 1, at, cols]
                if h_re is None:
                    h_re, h_im = p_re, p_im
                else:
                    h_re, h_im = r_re * h_re - r_im * h_im + p_re, r_re * h_im + r_im * h_re + p_im
            ends[d, 0, :, cols] = h_re
            ends[d, 1, :, cols] = h_im

    sub = iota((SUB, total), 0)
    message = []
    for d in range(2):
        power = tuple(rate_all[d])
        taken = 1
        while taken < steps:
            power = square(*power)
            taken *= 2
        a = (power[0] * kept[d], power[1] * kept[d])
        b = (ends[d, 0] * kept[d], ends[d, 1] * kept[d])

        def moved(value, by, fill):
            shift = by if d == 0 else SUB - by
            fine = sub >= by if d == 0 else sub < SUB - by
            return jnp.where(fine, pltpu.roll(value, shift, 0), fill)

        by = 1
        while by < SUB:
            pa = (moved(a[0], by, 1.0), moved(a[1], by, 0.0))
            pb = (moved(b[0], by, 0.0), moved(b[1], by, 0.0))
            b = plus(times(a, pb), b)
            a = times(a, pa)
            by *= 2
        before[d, 0] = moved(a[0], 1, 1.0)
        before[d, 1] = moved(a[1], 1, 0.0)
        before[d, 2] = moved(b[0], 1, 0.0)
        before[d, 3] = moved(b[1], 1, 0.0)
        edge = slice(SUB - 1, SUB) if d == 0 else slice(0, 1)
        message.append(((a[0][edge], a[1][edge]), (b[0][edge], b[1][edge])))

    pl.semaphore_wait(barrier, n_dev - 1)
    carry = [None, None]
    scan_copies = []
    for stage in range(3):
        stride = SIDE**stage
        place = lax.rem(sp // stride, SIDE)
        rows = [part for d in range(2) for pairs in message[d] for part in pairs]
        block = jnp.concatenate(rows, axis=0)
        msg[stage] = block.astype(BF16)
        copies = []
        for k in range(1, SIDE):
            there = lax.rem(place + k, SIDE)
            copy = pltpu.make_async_remote_copy(
                src_ref=msg.at[stage],
                dst_ref=recv_ends.at[stage, place],
                send_sem=scan_send.at[stage * SIDE + k],
                recv_sem=scan_recv.at[stage * SIDE + k],
                device_id={"sp": sp + (there - place) * stride, "tp": tp},
                device_id_type=MESH,
            )
            copy.start()
            copies.append(copy)
        recv_ends[stage, place] = block.astype(BF16)
        if stage == 0:
            for s in range(2):
                for d in range(2):
                    for part in range(2):
                        rows = sets[s][3][d, part].reshape(width, states_of[s])
                        if part:
                            rows = -rows
                        for which, q, _, column, lanes in packs:
                            if which == s:
                                begin = 2 * column + part * lanes
                                leave[d, :, begin : begin + lanes] = spread(
                                    rows[q * LANES : (q + 1) * LANES], masks[s]
                                )
                gate_rows = gate_mix[s].astype(F32).reshape(width, channels)
                gate_mask = (iota((LANES, LANES), 0) // channels) == (iota((LANES, LANES), 1) // channels)
                for q in range(groups // per):
                    gates[s * (groups // per) + q] = spread(
                        gate_rows[q * LANES : (q + 1) * LANES], gate_mask
                    )
        for copy in copies:
            copy.wait_recv()
        scan_copies += copies
        fetched = [recv_ends[stage, j].astype(F32) for j in range(SIDE)]
        for d in range(2):
            one = jnp.ones((1, total), F32)
            zero = jnp.zeros((1, total), F32)
            pre_a, pre_b = (one, zero), (zero, zero)
            tot_a, tot_b = None, None
            for j in steps_of(SIDE, d):
                use = (j < place) if d == 0 else (j > place)
                parts = [fetched[j][4 * d + r : 4 * d + r + 1] for r in range(4)]
                a, b = tuple(parts[:2]), tuple(parts[2:])
                if tot_a is None:
                    tot_a, tot_b = a, b
                else:
                    tot_a, tot_b = times(a, tot_a), plus(times(a, tot_b), b)
                pre_a = tuple(jnp.where(use, new, old) for new, old in zip(tot_a, pre_a))
                pre_b = tuple(jnp.where(use, new, old) for new, old in zip(tot_b, pre_b))
            message[d] = (tot_a, tot_b)
            if carry[d] is None:
                carry[d] = (pre_a, pre_b)
            else:
                carry[d] = (times(carry[d][0], pre_a), plus(times(carry[d][0], pre_b), carry[d][1]))

    for d in range(2):
        c_re, c_im = carry[d][1]
        a_re, a_im = before[d, 0], before[d, 1]
        ends[d, 0] = a_re * c_re - a_im * c_im + before[d, 2]
        ends[d, 1] = a_re * c_im + a_im * c_re + before[d, 3]

    for index, (s, q, chan, column, lanes) in enumerate(packs):
        cols = slice(column, column + lanes)
        chans = slice(chan, chan + LANES)
        read = skip[s : s + 1, q * LANES : (q + 1) * LANES].astype(F32) * plain[:, chans]
        for d in range(2):
            r_re, r_im = rate_all[d][0][:, cols], rate_all[d][1][:, cols]
            h_re, h_im = ends[d, 0, :, cols], ends[d, 1, :, cols]
            held = None
            for step in steps_of(steps, d):
                at = slice(step * SUB, (step + 1) * SUB)
                p_re, p_im = push[d, 0, at, cols], push[d, 1, at, cols]
                h_re, h_im = r_re * h_re - r_im * h_im + p_re, r_re * h_im + r_im * h_re + p_im
                if held is None:
                    held = (h_re, h_im)
                else:
                    low = min(step, step + 1 if d else step - 1) * SUB
                    for part, new in enumerate((h_re, h_im)):
                        both = [held[part], new] if d == 0 else [new, held[part]]
                        states[d, low : low + 2 * SUB, part * lanes : (part + 1) * lanes] = (
                            jnp.concatenate(both, axis=0).astype(BF16)
                        )
                    held = None
            term = dot(
                states[d, :, : 2 * lanes], leave[d, :, 2 * column : 2 * column + 2 * lanes], ((1,), (1,))
            )
            read = read + shrink[d, :, chans] * term
        active = jax.nn.gelu(read, approximate=True)
        opened = jax.nn.sigmoid(dot(active.astype(BF16), gates[index]))
        woven[:, chans] = (active * opened).astype(BF16)

    half = tokens // 2
    halves[...] = dot(unweave, woven[...]).astype(BF16).reshape(halves.shape)
    swap = pltpu.make_async_remote_copy(
        src_ref=halves.at[1 - tp],
        dst_ref=pair.at[tp],
        send_sem=pair_sem.at[0],
        recv_sem=pair_sem.at[1],
        device_id={"sp": sp, "tp": 1 - tp},
        device_id_type=MESH,
    )
    swap.start()
    pair[tp] = halves[tp]
    picks = iota((2 * n_dev, half), 0) // 2
    slot = lax.rem(iota((2 * n_dev, half), 0), 2).astype(F32)
    named = [routes[k : k + 1, :] == picks for k in range(2)]
    any_named = ones_where(named[0] | named[1])
    upper = ones_where(iota((half, half), 0) < iota((half, half), 1), BF16)
    earlier = dot(any_named.astype(BF16), upper)
    chosen = earlier == slot
    spots = jnp.where(chosen, any_named, 0.0).astype(BF16)
    share_sum = route_weights[0:1, :] + route_weights[1:2, :]
    weight = sum(
        jnp.where(named[k] & chosen, route_weights[k : k + 1, :] / share_sum, 0.0) for k in range(2)
    )
    high = weight.astype(BF16)
    low = (weight - high.astype(F32)).astype(BF16)
    fetches[0].wait()
    swap.wait_recv()
    joined = jnp.concatenate(
        [pair[k, :, :width] for k in range(2)] + [pair[k, :, width:] for k in range(2)], axis=1
    ).astype(F32)
    scale = lax.rsqrt(jnp.mean(joined * joined, axis=1, keepdims=True) + epsilon)
    mixed = (joined * scale * mixer_gain[...]).astype(BF16)
    hidden1 = (residual[...].astype(F32) + dot(mixed, proj_v[...])).astype(BF16)
    hidden_wide = hidden1.astype(F32)
    normed = (
        hidden_wide
        * lax.rsqrt(jnp.mean(hidden_wide * hidden_wide, axis=1, keepdims=True) + epsilon)
        * ffn_gain[...]
    ).astype(BF16)
    sec[...] = dot(spots, normed).astype(BF16).reshape(sec.shape)

    def partner(k, flip):
        dz, dy, dx = k // (SIDE * SIDE), lax.rem(k // SIDE, SIDE), lax.rem(k, SIDE)
        z, y, x = sp // (SIDE * SIDE), lax.rem(sp // SIDE, SIDE), lax.rem(sp, SIDE)
        other = (
            lax.rem(z + dz, SIDE) * SIDE * SIDE + lax.rem(y + dy, SIDE) * SIDE + lax.rem(x + dx, SIDE)
        )
        return other, (tp if flip == 0 else 1 - tp)

    own = pltpu.make_async_copy(sec.at[mine], arrived.at[0, sp], self_sem.at[0])
    own.start()
    for flip in range(2):

        def send(k, _):
            other, side = partner(k, flip)
            pltpu.make_async_remote_copy(
                src_ref=sec.at[other * 2 + side],
                dst_ref=arrived.at[flip, sp],
                send_sem=send_sem.at[flip],
                recv_sem=recv_sem.at[flip],
                device_id={"sp": other, "tp": side},
                device_id_type=MESH,
            ).start()
            return 0

        lax.fori_loop(1 - flip, n_sp, send, 0)

    own.wait()
    for fetch in fetches[1:]:
        fetch.wait()
    experts_width = hidden_v.shape[1]
    tile = 256

    def wait_bytes(ref, count, sem):
        pltpu.make_async_copy(ref.at[pl.ds(0, count)], ref.at[pl.ds(0, count)], sem).wait()

    def halfway(begin, size):
        cols = pl.ds(begin, size)
        gate_val = dot(rows_v[...], gate_v[:, cols])
        up_val = dot(rows_v[...], up_v[:, cols])
        hidden_v[:, cols] = (jax.nn.silu(gate_val) * up_val).astype(BF16)

    for flip in range(2):
        wait_bytes(arrived.at[flip], n_sp - 1 + flip, recv_sem.at[flip])
        rows_v[...] = arrived[flip].reshape(rows_v.shape)

        def first(n, _):
            halfway(pl.multiple_of(n * tile, tile), tile)
            return 0

        whole = experts_width // tile
        lax.fori_loop(0, whole, first, 0)
        if experts_width % tile:
            halfway(whole * tile, experts_width % tile)

        def second(n, _):
            cols = pl.ds(pl.multiple_of(n * tile, tile), tile)
            value = dot(hidden_v[...], down_v[:, cols]).astype(BF16)
            served[flip, :, :, cols] = value.reshape(n_sp, 2, tile)
            return 0

        lax.fori_loop(0, served.shape[3] // tile, second, 0)

        def give(k, _):
            other, side = partner(k, flip)
            pltpu.make_async_remote_copy(
                src_ref=served.at[flip, other],
                dst_ref=returned.at[mine],
                send_sem=back_send.at[flip],
                recv_sem=back_recv,
                device_id={"sp": other, "tp": side},
                device_id_type=MESH,
            ).start()
            return 0

        lax.fori_loop(1 - flip, n_sp, give, 0)
        if flip == 0:
            own_back = pltpu.make_async_copy(served.at[0, sp], returned.at[mine], self_sem.at[1])
            own_back.start()

    own_back.wait()
    wait_bytes(returned, n_dev - 1, back_recv)
    back = returned[...].reshape(2 * n_dev, -1)
    summed = dot(high, back, ((0,), (0,))) + dot(low, back, ((0,), (0,)))
    out_ref[...] = (hidden_wide + summed).astype(BF16)

    for copy in scan_copies:
        copy.wait_send()
    swap.wait_send()
    for flip in range(2):
        wait_bytes(sec, n_sp - 1 + flip, send_sem.at[flip])
        wait_bytes(served.at[flip], n_sp - 1 + flip, back_send.at[flip])


def local(
    wide_inputs, narrow_inputs, wide_poles, narrow_poles, step_sizes, forget, wide_in_map,
    narrow_in_map, wide_out_map, narrow_out_map, skip_weight, gate_mix, residual, mixer_gain,
    out_proj, ffn_gain, routes, route_weights, gate_proj, up_proj, down_proj,
):
    n_sp = lax.axis_size("sp")
    n_dev = 2 * n_sp
    tokens, width = wide_inputs.shape
    groups = wide_in_map.shape[2]
    total = groups * (wide_in_map.shape[4] + narrow_in_map.shape[4])
    widest = LANES // wide_in_map.shape[3] * wide_in_map.shape[4]
    rows, model = residual.shape
    fe = gate_proj.shape[2]
    vmem = pl.BlockSpec(memory_space=pltpu.VMEM)
    hbm = pl.BlockSpec(memory_space=pl.ANY)
    dma = pltpu.SemaphoreType.DMA
    return pl.pallas_call(
        layer_kernel,
        out_shape=jax.ShapeDtypeStruct((rows, model), BF16),
        in_specs=[vmem] * 17 + [hbm] * 4,
        out_specs=vmem,
        scratch_shapes=[
            pltpu.VMEM(out_proj.shape, BF16),
            pltpu.VMEM((model, fe), BF16),
            pltpu.VMEM((model, fe), BF16),
            pltpu.VMEM((fe, model), BF16),
            pltpu.VMEM((2, 2, tokens, total), F32),
            pltpu.VMEM((2, tokens, 2 * width), BF16),
            pltpu.VMEM((2, tokens, 2 * width), F32),
            pltpu.VMEM((tokens, 2 * width), F32),
            pltpu.VMEM((2, LANES, 2 * total), BF16),
            pltpu.VMEM((2 * width // LANES, LANES, LANES), BF16),
            pltpu.VMEM((2, 2, SUB, total), F32),
            pltpu.VMEM((2, 4, SUB, total), F32),
            pltpu.VMEM((3, SIDE, SUB, total), BF16),
            pltpu.VMEM((3, SUB, total), BF16),
            pltpu.VMEM((2, tokens, 2 * widest), BF16),
            pltpu.VMEM((tokens, 2 * width), BF16),
            pltpu.VMEM((2, tokens // 2, 2 * width), BF16),
            pltpu.VMEM((2, tokens // 2, 2 * width), BF16),
            pltpu.VMEM((n_dev, 2, model), BF16),
            pltpu.VMEM((2, n_sp, 2, model), BF16),
            pltpu.VMEM((2 * n_sp, model), BF16),
            pltpu.VMEM((2 * n_sp, fe), BF16),
            pltpu.VMEM((2, n_sp, 2, model), BF16),
            pltpu.VMEM((n_dev, 2, model), BF16),
            dma((4,)), dma((3 * SIDE,)), dma((3 * SIDE,)), dma((2,)), dma((2,)), dma((2,)), dma((2,)),
            dma, dma((2,)),
        ],
        compiler_params=pltpu.CompilerParams(
            collective_id=0, has_side_effects=True, vmem_limit_bytes=60 * 1024 * 1024
        ),
        name="layer",
    )(
        wide_inputs, narrow_inputs, wide_poles, narrow_poles, step_sizes, forget, wide_in_map,
        narrow_in_map, wide_out_map, narrow_out_map, skip_weight, gate_mix, residual,
        mixer_gain.reshape(1, -1), ffn_gain.reshape(1, -1), routes.T, route_weights.T, out_proj,
        gate_proj, up_proj, down_proj,
    )


def solution(mesh):
    return jax.shard_map(
        local,
        mesh=mesh,
        in_specs=(
            P("sp", "tp"),
            P("sp", "tp"),
            P(None, None, "tp", None),
            P(None, None, "tp", None),
            P(None, None, "tp"),
            P(None, None, "tp", "sp"),
            P(None, None, "tp", None, None),
            P(None, None, "tp", None, None),
            P(None, None, "tp", None, None),
            P(None, None, "tp", None, None),
            P(None, "tp"),
            P(None, "tp", None, None),
            P(("sp", "tp"), None),
            P(),
            P(),
            P(),
            P(("sp", "tp"), None),
            P(("sp", "tp"), None),
            P(("sp", "tp"), None, None),
            P(("sp", "tp"), None, None),
            P(("sp", "tp"), None, None),
        ),
        out_specs=P(("sp", "tp"), None),
        check_vma=False,
    )
```

time: 167 us -> 63.5 us (0.38)
  blocking collectives: 26.6 us -> 0 us
  waiting for transfers between devices: 19.5 us -> 0 us
  matrix products: 18 us -> 0 us
  other arithmetic: 9.86 us -> 0 us
  Pallas kernels: 71.4 us -> 61.7 us
  starting transfers between devices: 9.33 us -> 0 us
  local copies, waits for them, and re-layouts: 10.8 us -> 1.67 us
    all_to_all x1 -> x0, blocking collectives: 26.6 us -> none  [local(): lax.all_to_all(sectioning.reshape(experts, capacity, width), ('sp', 'tp')...]
    all_to_all x2 -> x0, waiting for transfers between devices: 19.5 us -> none  [the longest x1 19.2 us: local(): lax.all_to_all(done.reshape(received.shape), ('sp', 'tp'), split_axis=0,...]
    dot_general x6 -> x0, matrix products: 18 us -> none  [the longest x1 8.19 us: local(): jnp.dot(expert_hidden, down_proj[0], preferred_element_type=jnp.float32)]
    pallas_call x3 -> x1, Pallas kernels: 71.4 us -> 61.7 us  [local(): pl.pallas_call(layer_kernel, out_shape=jax.ShapeDtypeStruct((rows, model)...]
    all_to_all x2 -> x0, starting transfers between devices: 9.33 us -> none  [the longest x1 4.9 us: local(): lax.all_to_all(set_out.reshape(n_tp, rows, -1), 'tp', split_axis=0, conca...]
    reshape x13 -> x0, local copies, waits for them, and re-layouts: 6.93 us -> none  [the longest x1 1.61 us: mixer(): mixed.reshape(steps, SUBLANES, -1)]
    mul x4 -> x0, other arithmetic: 3.27 us -> none  [the longest x2 1.64 us: entering_map(): factor_re * moved[:, 0] - factor_im * moved[:, 1]]
    concatenate x2 -> x0, other arithmetic: 1.82 us -> none  [the longest x1 0.93 us: mixer(): enter = jnp.concatenate([wide_enter, narrow_enter], axis=3)]
  transfers between devices with their start and end apart: 2 -> 0, of which waited for: 2 -> 0; matrix products, arithmetic and copies ran while one was open for 1% -> 0% of each run, Pallas kernels for 0% -> 0%
where the time goes in v1:
time: 63.5 us; the launch traced here: 63.3 us
  Pallas kernels  61.7 us (97%)
  local copies, waits for them, and re-layouts  1.67 us (3%)
    pallas_call x1, Pallas kernels, local(): pl.pallas_call(layer_kernel, out_shape=jax.ShapeDtypeStruct((rows, model)...  61.7 us
    unnamed x1, local copies, waits for them, and re-layouts  1.67 us

profile of v1, /device:TPU:1, one launch (start us, length us, event | category | flops | bytes accessed | tf_op | source)
XLA Modules:
  0.0 63.3 jit_solution(3471653934332548932)
XLA Ops:
  0.0 61.7 %layer.1 = bf16[64,2048]{1,0:T(8,128)(2,1)} custom-call(bf16[128,256]{1,0:T(8,128)(2,1)} %wide_u.1, bf16[128,256]{1,0:T(8,128)(2,1)} %narrow_u.1, f32[2,2,16,64]{3,2,1,0:T(8,128)} %wide_poles.1, f32[2,2,16,32]{3,2,1,0:T(8,128)} %narrow_poles.1, f32[2,2,16]{2,1,0:T(2,128)} %step_sizes.1, f32[2,2,16,128]{3,2,1,0:T(8,128)} %forget.1, ...), custom_call_target="tpu_custom_call" | custom-call | tf_op jit(solution)/shard_map/layer/pallas_call | solution.py:489
  61.7 1.7 %copy.23 = bf16[64,2048]{1,0:T(8,128)(2,1)} copy(bf16[64,2048]{1,0:T(8,128)(2,1)} %layer.1) | data formatting | bytes 524288

commit v2 on v1

--- a/solution.py
+++ b/solution.py
@@ -10,6 +10,7 @@
 epsilon = 1e-06
 SIDE = 4
 SUB = 8
+SMALL = 17
 LANES = 128
 EXACT = lax.Precision.HIGHEST
 F32 = jnp.float32
@@ -61,15 +62,29 @@
     return range(count) if direction == 0 else range(count - 1, -1, -1)
 
 
-def layer_kernel(
-    wide_u, narrow_u, wide_poles, narrow_poles, step_sizes, forget, wide_in, narrow_in, wide_out,
-    narrow_out, skip, gate_mix, residual, mixer_gain, ffn_gain, routes, route_weights, out_proj,
-    gate_proj, up_proj, down_proj,
-    out_ref,
+def layer_kernel(*refs):
+    sources, refs = refs[:SMALL], refs[SMALL:]
+    (out_proj, gate_proj, up_proj, down_proj, out_ref), refs = refs[:5], refs[5:]
+    staged, refs = refs[:SMALL], refs[SMALL:]
+    layer_body(sources, staged, out_proj, gate_proj, up_proj, down_proj, out_ref, *refs)
+
+
+def layer_body(
+    sources, staged, out_proj, gate_proj, up_proj, down_proj, out_ref,
     proj_v, gate_v, up_v, down_v, push, scaled, shrink, plain, leave, gates, ends, before, recv_ends,
     msg, states, woven, halves, pair, sec, arrived, rows_v, hidden_v, served, returned,
-    weight_sem, scan_send, scan_recv, pair_sem, send_sem, recv_sem, back_send, back_recv, self_sem,
+    weight_sem, scan_send, scan_recv, pair_sem, send_sem, recv_sem, back_send, back_recv, self_sem, small_sem,
 ):
+    (
+        wide_u, narrow_u, forget, wide_poles, narrow_poles, step_sizes, wide_in, narrow_in, wide_out,
+        narrow_out, gate_mix, skip, routes, route_weights, mixer_gain, ffn_gain, residual,
+    ) = staged
+    smalls = [
+        pltpu.make_async_copy(source, target, small_sem.at[i])
+        for i, (source, target) in enumerate(zip(sources, staged))
+    ]
+    for small in smalls:
+        small.start()
     n_sp = lax.axis_size("sp")
     sp = lax.axis_index("sp")
     tp = lax.axis_index("tp")
@@ -78,14 +93,18 @@
 
     barrier = pltpu.get_barrier_semaphore()
 
-    def greet(k, _):
-        other = lax.rem(mine + k, n_dev)
-        pl.semaphore_signal(
-            barrier, inc=1, device_id={"sp": other // 2, "tp": lax.rem(other, 2)}, device_id_type=MESH
-        )
-        return 0
-
-    lax.fori_loop(1, n_dev, greet, 0)
+    for stage in range(3):
+        stride = SIDE**stage
+        place = lax.rem(sp // stride, SIDE)
+        for k in range(1, SIDE):
+            there = lax.rem(place + k, SIDE)
+            pl.semaphore_signal(
+                barrier,
+                inc=1,
+                device_id={"sp": sp + (there - place) * stride, "tp": tp},
+                device_id_type=MESH,
+            )
+    pl.semaphore_signal(barrier, inc=1, device_id={"sp": sp, "tp": 1 - tp}, device_id_type=MESH)
     fetches = [
         pltpu.make_async_copy(source, target, weight_sem.at[i])
         for i, (source, target) in enumerate(
@@ -95,6 +114,8 @@
     for fetch in fetches:
         fetch.start()
 
+    for small in smalls[:8]:
+        small.wait()
     tokens = wide_u.shape[0]
     steps = tokens // SUB
     sets = (
@@ -232,7 +253,7 @@
         edge = slice(SUB - 1, SUB) if d == 0 else slice(0, 1)
         message.append(((a[0][edge], a[1][edge]), (b[0][edge], b[1][edge])))
 
-    pl.semaphore_wait(barrier, n_dev - 1)
+    pl.semaphore_wait(barrier, 3 * (SIDE - 1) + 1)
     carry = [None, None]
     scan_copies = []
     for stage in range(3):
@@ -256,6 +277,8 @@
             copies.append(copy)
         recv_ends[stage, place] = block.astype(BF16)
         if stage == 0:
+            for small in smalls[8:]:
+                small.wait()
             for s in range(2):
                 for d in range(2):
                     for part in range(2):
@@ -406,38 +429,17 @@
     own.wait()
     for fetch in fetches[1:]:
         fetch.wait()
-    experts_width = hidden_v.shape[1]
-    tile = 256
-
     def wait_bytes(ref, count, sem):
         pltpu.make_async_copy(ref.at[pl.ds(0, count)], ref.at[pl.ds(0, count)], sem).wait()
-
-    def halfway(begin, size):
-        cols = pl.ds(begin, size)
-        gate_val = dot(rows_v[...], gate_v[:, cols])
-        up_val = dot(rows_v[...], up_v[:, cols])
-        hidden_v[:, cols] = (jax.nn.silu(gate_val) * up_val).astype(BF16)
 
     for flip in range(2):
         wait_bytes(arrived.at[flip], n_sp - 1 + flip, recv_sem.at[flip])
         rows_v[...] = arrived[flip].reshape(rows_v.shape)
 
-        def first(n, _):
-            halfway(pl.multiple_of(n * tile, tile), tile)
-            return 0
-
-        whole = experts_width // tile
-        lax.fori_loop(0, whole, first, 0)
-        if experts_width % tile:
-            halfway(whole * tile, experts_width % tile)
-
-        def second(n, _):
-            cols = pl.ds(pl.multiple_of(n * tile, tile), tile)
-            value = dot(hidden_v[...], down_v[:, cols]).astype(BF16)
-            served[flip, :, :, cols] = value.reshape(n_sp, 2, tile)
-            return 0
-
-        lax.fori_loop(0, served.shape[3] // tile, second, 0)
+        gate_val = dot(rows_v[...], gate_v[...])
+        up_val = dot(rows_v[...], up_v[...])
+        hidden_v[...] = (jax.nn.silu(gate_val) * up_val).astype(BF16)
+        served[flip] = dot(hidden_v[...], down_v[...]).astype(BF16).reshape(served.shape[1:])
 
         def give(k, _):
             other, side = partner(k, flip)
@@ -483,15 +485,20 @@
     widest = LANES // wide_in_map.shape[3] * wide_in_map.shape[4]
     rows, model = residual.shape
     fe = gate_proj.shape[2]
-    vmem = pl.BlockSpec(memory_space=pltpu.VMEM)
-    hbm = pl.BlockSpec(memory_space=pl.ANY)
+    hbm = pl.BlockSpec(memory_space=pltpu.HBM)
+    smalls = (
+        wide_inputs, narrow_inputs, forget, wide_poles, narrow_poles, step_sizes, wide_in_map,
+        narrow_in_map, wide_out_map, narrow_out_map, gate_mix, skip_weight, routes.T,
+        route_weights.T, mixer_gain.reshape(1, -1), ffn_gain.reshape(1, -1), residual,
+    )
     dma = pltpu.SemaphoreType.DMA
-    return pl.pallas_call(
+    result = pl.pallas_call(
         layer_kernel,
         out_shape=jax.ShapeDtypeStruct((rows, model), BF16),
-        in_specs=[vmem] * 17 + [hbm] * 4,
-        out_specs=vmem,
-        scratch_shapes=[
+        in_specs=[hbm] * (SMALL + 4),
+        out_specs=pl.BlockSpec(memory_space=pltpu.VMEM),
+        scratch_shapes=[pltpu.VMEM(each.shape, each.dtype) for each in smalls]
+        + [
             pltpu.VMEM(out_proj.shape, BF16),
             pltpu.VMEM((model, fe), BF16),
             pltpu.VMEM((model, fe), BF16),
@@ -517,18 +524,14 @@
             pltpu.VMEM((2, n_sp, 2, model), BF16),
             pltpu.VMEM((n_dev, 2, model), BF16),
             dma((4,)), dma((3 * SIDE,)), dma((3 * SIDE,)), dma((2,)), dma((2,)), dma((2,)), dma((2,)),
-            dma, dma((2,)),
+            dma, dma((2,)), dma((SMALL,)),
         ],
         compiler_params=pltpu.CompilerParams(
             collective_id=0, has_side_effects=True, vmem_limit_bytes=60 * 1024 * 1024
         ),
         name="layer",
-    )(
-        wide_inputs, narrow_inputs, wide_poles, narrow_poles, step_sizes, forget, wide_in_map,
-        narrow_in_map, wide_out_map, narrow_out_map, skip_weight, gate_mix, residual,
-        mixer_gain.reshape(1, -1), ffn_gain.reshape(1, -1), routes.T, route_weights.T, out_proj,
-        gate_proj, up_proj, down_proj,
-    )
+    )(*smalls, out_proj, gate_proj, up_proj, down_proj)
+    return result
 
 
 def solution(mesh):

time: 63.5 us -> 56.6 us (0.89)
  Pallas kernels: 61.7 us -> 54.7 us
    pallas_call x1, Pallas kernels: 61.7 us -> 54.7 us  [local(): pl.pallas_call(layer_kernel, out_shape=jax.ShapeDtypeStruct((rows, model)...]
where the time goes in v2:
time: 56.6 us; the launch traced here: 56.4 us
  Pallas kernels  54.7 us (97%)
  local copies, waits for them, and re-layouts  1.67 us (3%)
    pallas_call x1, Pallas kernels, local(): pl.pallas_call(layer_kernel, out_shape=jax.ShapeDtypeStruct((rows, model)...  54.7 us
    unnamed x1, local copies, waits for them, and re-layouts  1.67 us

profile of v2, /device:TPU:1, one launch (start us, length us, event | category | flops | bytes accessed | tf_op | source)
XLA Modules:
  0.0 56.4 jit_solution(2918496273526030528)
XLA Ops:
  0.0 54.7 %layer.1 = bf16[64,2048]{1,0:T(8,128)(2,1)} custom-call(bf16[128,256]{1,0:T(8,128)(2,1)} %refs_0_.1, bf16[128,256]{1,0:T(8,128)(2,1)} %refs_1_.1, f32[2,2,16,128]{3,2,1,0:T(8,128)} %refs_2_.1, f32[2,2,16,64]{3,2,1,0:T(8,128)} %refs_3_.1, f32[2,2,16,32]{3,2,1,0:T(8,128)} %refs_4_.1, f32[2,2,16]{2,1,0:T(2,128)} %refs_5_.1, f32[2,2,16,16,64]{4,3,2,1,0:T(8,128)} %refs_6_.1, ...), custom_call_target="tpu_custom_call" | custom-call | tf_op jit(solution)/shard_map/layer/pallas_call | solution.py:495
  54.8 1.7 %copy.23 = bf16[64,2048]{1,0:T(8,128)(2,1)} copy(bf16[64,2048]{1,0:T(8,128)(2,1)} %layer.1) | data formatting | bytes 524288

commit v3 on v2

--- a/solution.py
+++ b/solution.py
@@ -88,8 +88,6 @@
     n_sp = lax.axis_size("sp")
     sp = lax.axis_index("sp")
     tp = lax.axis_index("tp")
-    mine = sp * 2 + tp
-    n_dev = n_sp * 2
 
     barrier = pltpu.get_barrier_semaphore()
 
@@ -111,7 +109,7 @@
             ((out_proj, proj_v), (gate_proj.at[0], gate_v), (up_proj.at[0], up_v), (down_proj.at[0], down_v))
         )
     ]
-    for fetch in fetches:
+    for fetch in fetches[:2]:
         fetch.start()
 
     for small in smalls[:8]:
@@ -150,7 +148,7 @@
         lane < bases[1], lane // states_of[0], groups + (lane - bases[1]) // states_of[1]
     )
     to_lane = ones_where(iota((2 * groups, total), 0) == owner)
-    kept = []
+    kept, kept_all = [], []
     for d in range(2):
         flat = forget[d].reshape(2 * groups, tokens)
         lost = dot(reach[d], flat, ((1,), (1,)), EXACT)
@@ -158,7 +156,9 @@
         shrink[d] = jnp.exp(-wide)
         scaled[d] = (plain[...] * jnp.exp(wide)).astype(BF16)
         last = lost[tokens - SUB :] if d == 0 else lost[:SUB]
-        kept.append(jnp.exp(-dot(last, to_lane, precision=EXACT)))
+        fall = dot(last, to_lane, precision=EXACT)
+        kept.append(jnp.exp(-fall))
+        kept_all.append(jnp.exp(-jnp.sum(fall, axis=0, keepdims=True)))
 
     masks = [
         (iota((LANES, per * st), 0) // channels) == (iota((LANES, per * st), 1) // st) for st in states_of
@@ -224,7 +224,11 @@
             ends[d, 1, :, cols] = h_im
 
     sub = iota((SUB, total), 0)
-    message = []
+    message, powers = [], []
+    folds = total // LANES
+
+    def fold(value):
+        return jnp.concatenate([value[:, i * LANES : (i + 1) * LANES] for i in range(folds)], axis=0)
     for d in range(2):
         power = tuple(rate_all[d])
         taken = 1
@@ -251,7 +255,13 @@
         before[d, 2] = moved(b[0], 1, 0.0)
         before[d, 3] = moved(b[1], 1, 0.0)
         edge = slice(SUB - 1, SUB) if d == 0 else slice(0, 1)
-        message.append(((a[0][edge], a[1][edge]), (b[0][edge], b[1][edge])))
+        message.append((fold(kept_all[d]), (fold(b[0][edge]), fold(b[1][edge]))))
+        stride_power = tuple(fold(part) for part in rate_all[d])
+        taken = 1
+        while taken < tokens:
+            stride_power = square(*stride_power)
+            taken *= 2
+        powers.append(stride_power)
 
     pl.semaphore_wait(barrier, 3 * (SIDE - 1) + 1)
     carry = [None, None]
@@ -259,8 +269,7 @@
     for stage in range(3):
         stride = SIDE**stage
         place = lax.rem(sp // stride, SIDE)
-        rows = [part for d in range(2) for pairs in message[d] for part in pairs]
-        block = jnp.concatenate(rows, axis=0)
+        block = jnp.concatenate([part for k, b in message for part in (k, b[0], b[1])], axis=0)
         msg[stage] = block.astype(BF16)
         copies = []
         for k in range(1, SIDE):
@@ -276,6 +285,8 @@
             copy.start()
             copies.append(copy)
         recv_ends[stage, place] = block.astype(BF16)
+        if stage < 2:
+            fetches[2 + stage].start()
         if stage == 0:
             for small in smalls[8:]:
                 small.wait()
@@ -302,28 +313,32 @@
         scan_copies += copies
         fetched = [recv_ends[stage, j].astype(F32) for j in range(SIDE)]
         for d in range(2):
-            one = jnp.ones((1, total), F32)
-            zero = jnp.zeros((1, total), F32)
+            one = jnp.ones((folds, LANES), F32)
+            zero = jnp.zeros((folds, LANES), F32)
             pre_a, pre_b = (one, zero), (zero, zero)
-            tot_a, tot_b = None, None
+            run_a, tot_k, tot_b = None, None, None
             for j in steps_of(SIDE, d):
                 use = (j < place) if d == 0 else (j > place)
-                parts = [fetched[j][4 * d + r : 4 * d + r + 1] for r in range(4)]
-                a, b = tuple(parts[:2]), tuple(parts[2:])
-                if tot_a is None:
-                    tot_a, tot_b = a, b
+                begin = 3 * d * folds
+                k, b_re, b_im = (fetched[j][begin + r * folds : begin + (r + 1) * folds] for r in range(3))
+                a, b = (powers[d][0] * k, powers[d][1] * k), (b_re, b_im)
+                if tot_b is None:
+                    run_a, tot_k, tot_b = a, k, b
                 else:
-                    tot_a, tot_b = times(a, tot_a), plus(times(a, tot_b), b)
-                pre_a = tuple(jnp.where(use, new, old) for new, old in zip(tot_a, pre_a))
+                    run_a, tot_k, tot_b = times(a, run_a), k * tot_k, plus(times(a, tot_b), b)
+                pre_a = tuple(jnp.where(use, new, old) for new, old in zip(run_a, pre_a))
                 pre_b = tuple(jnp.where(use, new, old) for new, old in zip(tot_b, pre_b))
-            message[d] = (tot_a, tot_b)
+            message[d] = (tot_k, tot_b)
+            powers[d] = square(*square(*powers[d]))
             if carry[d] is None:
                 carry[d] = (pre_a, pre_b)
             else:
                 carry[d] = (times(carry[d][0], pre_a), plus(times(carry[d][0], pre_b), carry[d][1]))
 
     for d in range(2):
-        c_re, c_im = carry[d][1]
+        c_re, c_im = (
+            jnp.concatenate([part[i : i + 1] for i in range(folds)], axis=1) for part in carry[d][1]
+        )
         a_re, a_im = before[d, 0], before[d, 1]
         ends[d, 0] = a_re * c_re - a_im * c_im + before[d, 2]
         ends[d, 1] = a_re * c_im + a_im * c_re + before[d, 3]
@@ -370,20 +385,32 @@
     )
     swap.start()
     pair[tp] = halves[tp]
-    picks = iota((2 * n_dev, half), 0) // 2
-    slot = lax.rem(iota((2 * n_dev, half), 0), 2).astype(F32)
-    named = [routes[k : k + 1, :] == picks for k in range(2)]
-    any_named = ones_where(named[0] | named[1])
+
+    def partner(k, flip, sign):
+        m = lax.rem(k, n_sp // 2)
+        dz, dy = m // (2 * SIDE), lax.rem(m // 2, SIDE)
+        dx = 2 * lax.rem(m, 2) + lax.rem(dz + dy + k // (n_sp // 2), 2)
+        z, y, x = sp // (SIDE * SIDE), lax.rem(sp // SIDE, SIDE), lax.rem(sp, SIDE)
+        z, y, x = (lax.rem(at + sign * by + SIDE, SIDE) for at, by in ((z, dz), (y, dy), (x, dx)))
+        return z * SIDE * SIDE + y * SIDE + x, (tp if flip == 0 else 1 - tp)
+
     upper = ones_where(iota((half, half), 0) < iota((half, half), 1), BF16)
-    earlier = dot(any_named.astype(BF16), upper)
-    chosen = earlier == slot
-    spots = jnp.where(chosen, any_named, 0.0).astype(BF16)
     share_sum = route_weights[0:1, :] + route_weights[1:2, :]
-    weight = sum(
-        jnp.where(named[k] & chosen, route_weights[k : k + 1, :] / share_sum, 0.0) for k in range(2)
-    )
-    high = weight.astype(BF16)
-    low = (weight - high.astype(F32)).astype(BF16)
+    line = iota((2 * n_sp, half), 0)
+    slot = lax.rem(line, 2).astype(F32)
+    spots, highs, lows = [], [], []
+    for flip in range(2):
+        other, side = partner(line // 2, flip, 1)
+        picks = other * 2 + side
+        named = [routes[k : k + 1, :] == picks for k in range(2)]
+        any_named = ones_where(named[0] | named[1])
+        chosen = dot(any_named.astype(BF16), upper) == slot
+        spots.append(jnp.where(chosen, any_named, 0.0).astype(BF16))
+        weight = sum(
+            jnp.where(named[k] & chosen, route_weights[k : k + 1, :] / share_sum, 0.0) for k in range(2)
+        )
+        highs.append(weight.astype(BF16))
+        lows.append((weight - highs[flip].astype(F32)).astype(BF16))
     fetches[0].wait()
     swap.wait_recv()
     joined = jnp.concatenate(
@@ -398,25 +425,17 @@
         * lax.rsqrt(jnp.mean(hidden_wide * hidden_wide, axis=1, keepdims=True) + epsilon)
         * ffn_gain[...]
     ).astype(BF16)
-    sec[...] = dot(spots, normed).astype(BF16).reshape(sec.shape)
-
-    def partner(k, flip):
-        dz, dy, dx = k // (SIDE * SIDE), lax.rem(k // SIDE, SIDE), lax.rem(k, SIDE)
-        z, y, x = sp // (SIDE * SIDE), lax.rem(sp // SIDE, SIDE), lax.rem(sp, SIDE)
-        other = (
-            lax.rem(z + dz, SIDE) * SIDE * SIDE + lax.rem(y + dy, SIDE) * SIDE + lax.rem(x + dx, SIDE)
-        )
-        return other, (tp if flip == 0 else 1 - tp)
-
-    own = pltpu.make_async_copy(sec.at[mine], arrived.at[0, sp], self_sem.at[0])
-    own.start()
     for flip in range(2):
+        sec[flip] = dot(spots[flip], normed).astype(BF16).reshape(sec.shape[1:])
+        if flip == 0:
+            own = pltpu.make_async_copy(sec.at[0, 0], arrived.at[0, 0], self_sem.at[0])
+            own.start()
 
         def send(k, _):
-            other, side = partner(k, flip)
+            other, side = partner(k, flip, 1)
             pltpu.make_async_remote_copy(
-                src_ref=sec.at[other * 2 + side],
-                dst_ref=arrived.at[flip, sp],
+                src_ref=sec.at[flip, k],
+                dst_ref=arrived.at[flip, k],
                 send_sem=send_sem.at[flip],
                 recv_sem=recv_sem.at[flip],
                 device_id={"sp": other, "tp": side},
@@ -442,12 +461,12 @@
         served[flip] = dot(hidden_v[...], down_v[...]).astype(BF16).reshape(served.shape[1:])
 
         def give(k, _):
-            other, side = partner(k, flip)
+            other, side = partner(k, flip, -1)
             pltpu.make_async_remote_copy(
-                src_ref=served.at[flip, other],
-                dst_ref=returned.at[mine],
+                src_ref=served.at[flip, k],
+                dst_ref=returned.at[flip, k],
                 send_sem=back_send.at[flip],
-                recv_sem=back_recv,
+                recv_sem=back_recv.at[flip],
                 device_id={"sp": other, "tp": side},
                 device_id_type=MESH,
             ).start()
@@ -455,20 +474,22 @@
 
         lax.fori_loop(1 - flip, n_sp, give, 0)
         if flip == 0:
-            own_back = pltpu.make_async_copy(served.at[0, sp], returned.at[mine], self_sem.at[1])
+            own_back = pltpu.make_async_copy(served.at[0, 0], returned.at[0, 0], self_sem.at[1])
             own_back.start()
 
     own_back.wait()
-    wait_bytes(returned, n_dev - 1, back_recv)
-    back = returned[...].reshape(2 * n_dev, -1)
-    summed = dot(high, back, ((0,), (0,))) + dot(low, back, ((0,), (0,)))
-    out_ref[...] = (hidden_wide + summed).astype(BF16)
+    result = hidden_wide
+    for flip in range(2):
+        wait_bytes(returned.at[flip], n_sp - 1 + flip, back_recv.at[flip])
+        back = returned[flip].reshape(2 * n_sp, -1)
+        result = result + dot(highs[flip], back, ((0,), (0,))) + dot(lows[flip], back, ((0,), (0,)))
+    out_ref[...] = result.astype(BF16)
 
     for copy in scan_copies:
         copy.wait_send()
     swap.wait_send()
     for flip in range(2):
-        wait_bytes(sec, n_sp - 1 + flip, send_sem.at[flip])
+        wait_bytes(sec.at[flip], n_sp - 1 + flip, send_sem.at[flip])
         wait_bytes(served.at[flip], n_sp - 1 + flip, back_send.at[flip])
 
 
@@ -478,7 +499,6 @@
     out_proj, ffn_gain, routes, route_weights, gate_proj, up_proj, down_proj,
 ):
     n_sp = lax.axis_size("sp")
-    n_dev = 2 * n_sp
     tokens, width = wide_inputs.shape
     groups = wide_in_map.shape[2]
     total = groups * (wide_in_map.shape[4] + narrow_in_map.shape[4])
@@ -511,20 +531,20 @@
             pltpu.VMEM((2 * width // LANES, LANES, LANES), BF16),
             pltpu.VMEM((2, 2, SUB, total), F32),
             pltpu.VMEM((2, 4, SUB, total), F32),
-            pltpu.VMEM((3, SIDE, SUB, total), BF16),
-            pltpu.VMEM((3, SUB, total), BF16),
+            pltpu.VMEM((3, SIDE, 6 * total // LANES, LANES), BF16),
+            pltpu.VMEM((3, 6 * total // LANES, LANES), BF16),
             pltpu.VMEM((2, tokens, 2 * widest), BF16),
             pltpu.VMEM((tokens, 2 * width), BF16),
             pltpu.VMEM((2, tokens // 2, 2 * width), BF16),
             pltpu.VMEM((2, tokens // 2, 2 * width), BF16),
-            pltpu.VMEM((n_dev, 2, model), BF16),
+            pltpu.VMEM((2, n_sp, 2, model), BF16),
             pltpu.VMEM((2, n_sp, 2, model), BF16),
             pltpu.VMEM((2 * n_sp, model), BF16),
             pltpu.VMEM((2 * n_sp, fe), BF16),
             pltpu.VMEM((2, n_sp, 2, model), BF16),
-            pltpu.VMEM((n_dev, 2, model), BF16),
+            pltpu.VMEM((2, n_sp, 2, model), BF16),
             dma((4,)), dma((3 * SIDE,)), dma((3 * SIDE,)), dma((2,)), dma((2,)), dma((2,)), dma((2,)),
-            dma, dma((2,)), dma((SMALL,)),
+            dma((2,)), dma((2,)), dma((SMALL,)),
         ],
         compiler_params=pltpu.CompilerParams(
             collective_id=0, has_side_effects=True, vmem_limit_bytes=60 * 1024 * 1024

time: 56.6 us -> 56.9 us (level)
  no operation moved by 1% of the time
where the time goes in v3:
time: 56.9 us; the launch traced here: 56.8 us
  Pallas kernels  55.1 us (97%)
  local copies, waits for them, and re-layouts  1.67 us (3%)
    pallas_call x1, Pallas kernels, local(): pl.pallas_call(layer_kernel, out_shape=jax.ShapeDtypeStruct((rows, model)...  55.1 us
    unnamed x1, local copies, waits for them, and re-layouts  1.67 us

profile of v3, /device:TPU:1, one launch (start us, length us, event | category | flops | bytes accessed | tf_op | source)
XLA Modules:
  0.0 56.8 jit_solution(12874933776045603791)
XLA Ops:
  0.0 55.1 %layer.1 = bf16[64,2048]{1,0:T(8,128)(2,1)} custom-call(bf16[128,256]{1,0:T(8,128)(2,1)} %refs_0_.1, bf16[128,256]{1,0:T(8,128)(2,1)} %refs_1_.1, f32[2,2,16,128]{3,2,1,0:T(8,128)} %refs_2_.1, f32[2,2,16,64]{3,2,1,0:T(8,128)} %refs_3_.1, f32[2,2,16,32]{3,2,1,0:T(8,128)} %refs_4_.1, f32[2,2,16]{2,1,0:T(2,128)} %refs_5_.1, f32[2,2,16,16,64]{4,3,2,1,0:T(8,128)} %refs_6_.1, ...), custom_call_target="tpu_custom_call" | custom-call | tf_op jit(solution)/shard_map/layer/pallas_call | solution.py:515
  55.1 1.7 %copy.23 = bf16[64,2048]{1,0:T(8,128)(2,1)} copy(bf16[64,2048]{1,0:T(8,128)(2,1)} %layer.1) | data formatting | bytes 524288

commit v4 on v3

--- a/solution.py
+++ b/solution.py
@@ -432,6 +432,7 @@
             own.start()
 
         def send(k, _):
+            k = n_sp - 1 - k if flip else n_sp - k
             other, side = partner(k, flip, 1)
             pltpu.make_async_remote_copy(
                 src_ref=sec.at[flip, k],
@@ -461,6 +462,7 @@
         served[flip] = dot(hidden_v[...], down_v[...]).astype(BF16).reshape(served.shape[1:])
 
         def give(k, _):
+            k = n_sp - 1 - k if flip else n_sp - k
             other, side = partner(k, flip, -1)
             pltpu.make_async_remote_copy(
                 src_ref=served.at[flip, k],

time: 56.9 us -> 54.8 us (0.963)
  Pallas kernels: 55.1 us -> 53 us
    pallas_call x1, Pallas kernels: 55.1 us -> 53 us  [local(): pl.pallas_call(layer_kernel, out_shape=jax.ShapeDtypeStruct((rows, model)...]
where the time goes in v4:
time: 54.8 us; the launch traced here: 54.7 us
  Pallas kernels  53 us (97%)
  local copies, waits for them, and re-layouts  1.67 us (3%)
    pallas_call x1, Pallas kernels, local(): pl.pallas_call(layer_kernel, out_shape=jax.ShapeDtypeStruct((rows, model)...  53 us
    unnamed x1, local copies, waits for them, and re-layouts  1.67 us

profile of v4, /device:TPU:1, one launch (start us, length us, event | category | flops | bytes accessed | tf_op | source)
XLA Modules:
  0.0 54.7 jit_solution(639709716346772487)
XLA Ops:
  0.0 53.0 %layer.1 = bf16[64,2048]{1,0:T(8,128)(2,1)} custom-call(bf16[128,256]{1,0:T(8,128)(2,1)} %refs_0_.1, bf16[128,256]{1,0:T(8,128)(2,1)} %refs_1_.1, f32[2,2,16,128]{3,2,1,0:T(8,128)} %refs_2_.1, f32[2,2,16,64]{3,2,1,0:T(8,128)} %refs_3_.1, f32[2,2,16,32]{3,2,1,0:T(8,128)} %refs_4_.1, f32[2,2,16]{2,1,0:T(2,128)} %refs_5_.1, f32[2,2,16,16,64]{4,3,2,1,0:T(8,128)} %refs_6_.1, ...), custom_call_target="tpu_custom_call" | custom-call | tf_op jit(solution)/shard_map/layer/pallas_call | solution.py:517
  53.0 1.7 %copy.23 = bf16[64,2048]{1,0:T(8,128)(2,1)} copy(bf16[64,2048]{1,0:T(8,128)(2,1)} %layer.1) | data formatting | bytes 524288

commit v5 on v4

--- a/solution.py
+++ b/solution.py
@@ -384,7 +384,6 @@
         device_id_type=MESH,
     )
     swap.start()
-    pair[tp] = halves[tp]
 
     def partner(k, flip, sign):
         m = lax.rem(k, n_sp // 2)
@@ -412,13 +411,22 @@
         highs.append(weight.astype(BF16))
         lows.append((weight - highs[flip].astype(F32)).astype(BF16))
     fetches[0].wait()
+
+    def projected(side, block):
+        wide = pl.ds(pl.multiple_of(side * width, width), width)
+        narrow = pl.ds(pl.multiple_of((2 + side) * width, width), width)
+        values = block.astype(F32)
+        gain = jnp.concatenate([mixer_gain[:, wide], mixer_gain[:, narrow]], axis=1)
+        scaled_by = (values * gain).astype(BF16)
+        product = dot(scaled_by[:, :width], proj_v[wide, :]) + dot(scaled_by[:, width:], proj_v[narrow, :])
+        return product, jnp.sum(values * values, axis=1, keepdims=True)
+
+    own_product, own_square = projected(tp, halves[tp])
     swap.wait_recv()
-    joined = jnp.concatenate(
-        [pair[k, :, :width] for k in range(2)] + [pair[k, :, width:] for k in range(2)], axis=1
-    ).astype(F32)
-    scale = lax.rsqrt(jnp.mean(joined * joined, axis=1, keepdims=True) + epsilon)
-    mixed = (joined * scale * mixer_gain[...]).astype(BF16)
-    hidden1 = (residual[...].astype(F32) + dot(mixed, proj_v[...])).astype(BF16)
+    their_product, their_square = projected(1 - tp, pair[1 - tp])
+    scale = lax.rsqrt((own_square + their_square) / (4 * width) + epsilon)
+    product = (own_product + their_product) * scale
+    hidden1 = (residual[...].astype(F32) + product).astype(BF16)
     hidden_wide = hidden1.astype(F32)
     normed = (
         hidden_wide

time: 54.8 us -> 54.7 us (level)
  no operation moved by 1% of the time
where the time goes in v5:
time: 54.7 us; the launch traced here: 54.5 us
  Pallas kernels  52.9 us (97%)
  local copies, waits for them, and re-layouts  1.67 us (3%)
    pallas_call x1, Pallas kernels, local(): pl.pallas_call(layer_kernel, out_shape=jax.ShapeDtypeStruct((rows, model)...  52.9 us
    unnamed x1, local copies, waits for them, and re-layouts  1.67 us

profile of v5, /device:TPU:1, one launch (start us, length us, event | category | flops | bytes accessed | tf_op | source)
XLA Modules:
  0.0 54.5 jit_solution(1775760416037565962)
XLA Ops:
  0.0 52.9 %layer.1 = bf16[64,2048]{1,0:T(8,128)(2,1)} custom-call(bf16[128,256]{1,0:T(8,128)(2,1)} %refs_0_.1, bf16[128,256]{1,0:T(8,128)(2,1)} %refs_1_.1, f32[2,2,16,128]{3,2,1,0:T(8,128)} %refs_2_.1, f32[2,2,16,64]{3,2,1,0:T(8,128)} %refs_3_.1, f32[2,2,16,32]{3,2,1,0:T(8,128)} %refs_4_.1, f32[2,2,16]{2,1,0:T(2,128)} %refs_5_.1, f32[2,2,16,16,64]{4,3,2,1,0:T(8,128)} %refs_6_.1, ...), custom_call_target="tpu_custom_call" | custom-call | tf_op jit(solution)/shard_map/layer/pallas_call | solution.py:525
  52.9 1.7 %copy.23 = bf16[64,2048]{1,0:T(8,128)(2,1)} copy(bf16[64,2048]{1,0:T(8,128)(2,1)} %layer.1) | data formatting | bytes 524288
